TPU v7x, 256 devices: a whole 4x4x8 slice. The times are simulated.
256 devices in a mesh: ep: 16 (over y, x), tp: 16 (over z, core).
Axes of the slice: x: 4, y: 4, z: 8, core: 2. Of those that a mesh axis runs over, the one named last changes fastest.
Arguments:
- mix_tokens: bfloat16 [16384, 1, 1024], P(('ep', 'tp')), may hold values from -6 to 6
- mix_gain: float32 [1024], replicated, may hold values from 0.1 to 1.9
- w_query: bfloat16 [1024, 1024], replicated, may hold values from -0.1875 to 0.1875
- w_key: bfloat16 [1024, 256], replicated, may hold values from -0.1875 to 0.1875
- w_value: bfloat16 [1024, 256], replicated, may hold values from -0.1875 to 0.1875
- query_gain: float32 [64], replicated, may hold values from 1.2 to 14
- key_gain: float32 [64], replicated, may hold values from 1.2 to 14
- w_out: bfloat16 [1024, 1024], replicated, may hold values from -0.1875 to 0.1875
- expert_tokens: bfloat16 [32768, 1024], P(('ep', 'tp')), may hold values from -6 to 6
- expert_gain: float32 [1024], replicated, may hold values from 0.1 to 1.9
- route_ids: int32 [32768, 2], P(('ep', 'tp')), may hold values from 0 to 31, all different within a row; in each aligned block of 128 rows (0 to 127, 128 to 255, ...) at most 9 rows name the same one
- route_weights: float32 [32768, 2], P(('ep', 'tp')), may hold values from 0.1 to 1
- w_gate: bfloat16 [32, 1024, 4096], P('ep', None, 'tp'), may hold values from -0.1875 to 0.1875
- w_up: bfloat16 [32, 1024, 4096], P('ep', None, 'tp'), may hold values from -0.1875 to 0.1875
- w_down: bfloat16 [32, 4096, 1024], P('ep', 'tp'), may hold values from -0.09375 to 0.09375
Outputs:
- mix_out: bfloat16 [16384, 1, 1024], P(('ep', 'tp'))
- experts_out: bfloat16 [32768, 1024], P(('ep', 'tp'))
Inputs may be any that keep to these rules, and one draw needn't show every extreme that they name: `route_ids`: each row names 2 different experts. Among the rows of one device no expert is named more than 9 times, and in every draw some expert is named exactly 9 times by the rows of some device.
All inputs are finite; a program needn't handle non-finite values.
Results may differ from a plain program's by a relative error of at most 0.018.
The roundings to bfloat16 on the way count: a program that leaves them out, or rounds other values in their place, can miss the bound.
Values may be sent and summed in bfloat16 or wider, within the bound.
A program may use at most 128 MiB of HBM per device.

v0:
```python
import math
import jax
import jax.numpy as jnp
from jax import lax
from jax.sharding import PartitionSpec as P

HEAD = 64
GRID_W = 64
epsilon = 1e-06


def normalize(values, gain_vec):
    widened = values.astype(jnp.float32)
    return (
        widened
        * lax.rsqrt(jnp.mean(widened * widened, axis=-1, keepdims=True) + epsilon)
        * gain_vec
    )


def angle_tables(positions, head_size):
    quarter = head_size // 4
    frequency = 10000.0 ** (-jnp.arange(quarter, dtype=jnp.float32) / quarter)
    grid_pos = jnp.stack([positions // GRID_W, positions % GRID_W], axis=-1).astype(jnp.float32)
    angles = grid_pos[:, :, None] * frequency[None, None, :]
    return (jnp.cos(angles), jnp.sin(angles))


def turn(values, cosine_table, sine_table):
    shaped = values.shape
    quarter = shaped[-1] // 4
    leading = (shaped[0],) + (1,) * (len(shaped) - 2) + (2, quarter)
    cosine_table = cosine_table.reshape(leading)
    sine_table = sine_table.reshape(leading)
    halves = values.reshape(shaped[:-1] + (2, 2, quarter))
    first_part = halves[..., 0, :]
    second_part = halves[..., 1, :]
    turned = jnp.stack(
        [
            first_part * cosine_table - second_part * sine_table,
            first_part * sine_table + second_part * cosine_table,
        ],
        axis=-2,
    )
    return turned.reshape(shaped)


def attend(queries, fold_state, key_piece):
    key_rows = key_piece.shape[0]
    block_rows = math.gcd(key_rows, 1024)
    blocks = key_piece.reshape((key_rows // block_rows, block_rows) + key_piece.shape[1:])
    score_scale = HEAD ** (-0.5)

    def step_block(carried, block_keys):
        running_max, totals, accumulated = carried
        keys_part = block_keys[..., :HEAD]
        values_part = block_keys[..., HEAD:]
        scores = (
            jnp.einsum("qshd,ksd->qshk", queries, keys_part, preferred_element_type=jnp.float32)
            * score_scale
        )
        new_max = jnp.maximum(running_max, jnp.max(scores, axis=-1))
        shrink = jnp.exp(running_max - new_max)
        raised = jnp.exp(scores - new_max[..., None])
        totals = totals * shrink + jnp.sum(raised, axis=-1)
        accumulated = accumulated * shrink[..., None] + jnp.einsum(
            "qshk,ksd->qshd",
            raised.astype(jnp.bfloat16),
            values_part,
            preferred_element_type=jnp.float32,
        )
        return ((new_max, totals, accumulated), None)

    return lax.scan(step_block, fold_state, blocks)[0]


def mixer_half(mix_tokens, mix_gain, w_query, w_key, w_value, query_gain, key_gain, w_out):
    tp_count = lax.axis_size("tp")
    seq_rows, sequences, model_width = mix_tokens.shape
    head_count = w_query.shape[1] // HEAD
    key_heads = w_key.shape[1] // HEAD
    local_heads = head_count // tp_count
    normed = normalize(mix_tokens, mix_gain).astype(jnp.bfloat16)
    queries = jnp.dot(normed, w_query, preferred_element_type=jnp.float32).astype(jnp.bfloat16)
    keys_raw = jnp.dot(normed, w_key, preferred_element_type=jnp.float32).astype(jnp.bfloat16)
    values = jnp.dot(normed, w_value, preferred_element_type=jnp.float32).astype(jnp.bfloat16)
    queries = queries.reshape(seq_rows, sequences, tp_count, local_heads * HEAD)
    key_value = jnp.concatenate(
        [
            keys_raw.reshape(seq_rows, sequences, key_heads, HEAD),
            values.reshape(seq_rows, sequences, key_heads, HEAD),
        ],
        axis=-1,
    )
    key_value = jnp.repeat(key_value, tp_count // key_heads, axis=2)
    packed = jnp.concatenate([queries, key_value], axis=-1)
    arrived = lax.all_to_all(packed, "tp", split_axis=2, concat_axis=0, tiled=True)
    span_rows = arrived.shape[0]
    positions = lax.axis_index("ep") * span_rows + jnp.arange(span_rows, dtype=jnp.int32)
    cosine_table, sine_table = angle_tables(positions, HEAD)
    query_width = local_heads * HEAD
    own_queries = normalize(
        arrived[:, :, 0, :query_width].reshape(span_rows, sequences, local_heads, HEAD), query_gain
    )
    own_queries = turn(own_queries, cosine_table, sine_table).astype(jnp.bfloat16)
    own_keys = normalize(arrived[:, :, 0, query_width : query_width + HEAD], key_gain)
    own_keys = turn(own_keys, cosine_table, sine_table).astype(jnp.bfloat16)
    key_pairs = jnp.concatenate([own_keys, arrived[:, :, 0, query_width + HEAD :]], axis=-1)
    start_state = (
        jnp.full((span_rows, sequences, local_heads), -1e30, jnp.float32),
        jnp.zeros((span_rows, sequences, local_heads), jnp.float32),
        jnp.zeros((span_rows, sequences, local_heads, HEAD), jnp.float32),
    )
    running_max, totals, accumulated = attend(
        own_queries, start_state, lax.all_gather(key_pairs, "ep", axis=0, tiled=True)
    )
    mixed = (
        (accumulated / totals[..., None])
        .astype(jnp.bfloat16)
        .reshape(span_rows, sequences, query_width)
    )
    returned = lax.all_to_all(mixed, "tp", split_axis=0, concat_axis=2, tiled=True)
    return jnp.dot(returned, w_out, preferred_element_type=jnp.float32).astype(jnp.bfloat16)


def joint_hidden(w_gate, w_up, piece_rows):
    gate_act = jnp.einsum("rjd,jdf->rjf", piece_rows, w_gate, preferred_element_type=jnp.float32)
    up_act = jnp.einsum("rjd,jdf->rjf", piece_rows, w_up, preferred_element_type=jnp.float32)
    return (jax.nn.silu(gate_act) * up_act).astype(jnp.bfloat16)


def joint_down(hidden_all, w_down):
    group_sum = jnp.einsum(
        "rjf,jfd->rjd", hidden_all, w_down, preferred_element_type=jnp.float32
    ).astype(jnp.bfloat16)
    return lax.optimization_barrier(group_sum).astype(jnp.float32)


def expert_half(expert_tokens, expert_gain, route_ids, route_weights, w_gate, w_up, w_down):
    ep_count = lax.axis_size("ep")
    tok_count, model_width = expert_tokens.shape
    top_count = route_ids.shape[1]
    local_experts = w_gate.shape[0]
    expert_count = local_experts * ep_count
    capacity = tok_count * top_count * 9 // (8 * expert_count)
    slot_count = ep_count * capacity * local_experts
    normed = normalize(expert_tokens, expert_gain).astype(jnp.bfloat16)
    flat_ids = route_ids.reshape(-1)
    matches = (flat_ids[:, None] == jnp.arange(expert_count, dtype=jnp.int32)[None, :]).astype(
        jnp.int32
    )
    rank_ids = jnp.sum((jnp.cumsum(matches, axis=0) - 1) * matches, axis=1)
    slot_ids = (
        flat_ids // local_experts * capacity + rank_ids
    ) * local_experts + flat_ids % local_experts
    chosen = slot_ids.reshape(tok_count, top_count)
    dispatch = jnp.sum(
        (chosen[:, :, None] == jnp.arange(slot_count, dtype=jnp.int32)[None, None, :]).astype(
            jnp.bfloat16
        ),
        axis=1,
    )
    outgoing = lax.dot_general(
        dispatch, normed, (((0,), (0,)), ((), ())), preferred_element_type=jnp.float32
    )
    outgoing = outgoing.astype(jnp.bfloat16).reshape(ep_count, capacity, local_experts, model_width)
    incoming = lax.all_to_all(outgoing, "ep", split_axis=0, concat_axis=0, tiled=True)
    own_rows = ep_count * capacity
    incoming = incoming.reshape(own_rows, local_experts, model_width)
    hidden_all = joint_hidden(w_gate, w_up, lax.all_gather(incoming, "tp", axis=0, tiled=True))
    summed = lax.psum_scatter(
        joint_down(hidden_all, w_down).astype(jnp.bfloat16), "tp", scatter_dimension=0, tiled=True
    )
    expert_results = summed.reshape(ep_count, capacity, local_experts, model_width)
    returned = lax.all_to_all(
        expert_results, "ep", split_axis=0, concat_axis=0, tiled=True
    ).reshape(slot_count, model_width)
    picked = jnp.take(returned, slot_ids, axis=0).reshape(tok_count, top_count, model_width)
    combined = jnp.sum(route_weights[:, :, None] * picked.astype(jnp.float32), axis=1)
    return combined.astype(jnp.bfloat16)


def body(
    mix_tokens,
    mix_gain,
    w_query,
    w_key,
    w_value,
    query_gain,
    key_gain,
    w_out,
    expert_tokens,
    expert_gain,
    route_ids,
    route_weights,
    w_gate,
    w_up,
    w_down,
):
    mix_out = mixer_half(mix_tokens, mix_gain, w_query, w_key, w_value, query_gain, key_gain, w_out)
    experts_out = expert_half(
        expert_tokens, expert_gain, route_ids, route_weights, w_gate, w_up, w_down
    )
    return (mix_out, experts_out)


def solution(mesh):
    placed = (
        P(("ep", "tp"), None, None),
        P(),
        P(),
        P(),
        P(),
        P(),
        P(),
        P(),
        P(("ep", "tp"), None),
        P(),
        P(("ep", "tp"), None),
        P(("ep", "tp"), None),
        P("ep", None, "tp"),
        P("ep", None, "tp"),
        P("ep", "tp", None),
    )
    return jax.shard_map(
        body,
        mesh=mesh,
        in_specs=placed,
        out_specs=(P(("ep", "tp"), None, None), P(("ep", "tp"), None)),
        check_vma=False,
    )
```

profile of v0, /device:TPU:1, one launch (start us, length us, event | category | flops | bytes accessed | tf_op | source)
XLA Modules:
  0.0 339.7 jit_solution(8806245419591874709)
XLA Ops:
  11.5 1.3 convolution_convert_fusion
  13.0 18.7 %all_to_all.43 = bf16[16,9,2,1024]{3,2,1,0:T(2,128)(2,1)S(1)} all-to-all(bf16[16,9,2,1024]{3,2,1,0:T(2,128)(2,1)S(1)} %reshape.571), channel_id=1, replica_groups=mesh['ep'=16,'tp'=16] {'ep'}, dimensions={0} | all-to-all | bytes 1179648 | tf_op jit(solution)/shard_map/all_to_all | solution.py:167
  37.7 10.4 %all-to-all-start = ((bf16[64,1,16,192]{3,0,1,2:T(8,128)(2,1)}), bf16[64,1,16,192]{3,0,1,2:T(8,128)(2,1)S(1)}, u32[]{:S(2)}, u32[]{:S(2)}) async-start(bf16[64,1,16,192]{3,0,1,2:T(8,128)(2,1)} %pad_maximum_fusion), calls=%async_computation | async-start | bytes 1048576 | tf_op jit(solution)/shard_map/all_to_all | solution.py:97
  48.3 22.1 %all-to-all-done = bf16[64,1,16,192]{3,0,1,2:T(8,128)(2,1)S(1)} async-done(((bf16[64,1,16,192]{3,0,1,2:T(8,128)(2,1)}), bf16[64,1,16,192]{3,0,1,2:T(8,128)(2,1)S(1)}, u32[]{:S(2)}, u32[]{:S(2)}) %all-to-all-start) | async-done | bytes 393248 | tf_op jit(solution)/shard_map/all_to_all | solution.py:97
  77.2 28.6 %all-gather.5.cloned.1.call-done = bf16[2304,2,1024]{2,0,1:T(8,128)(2,1)} async-done(((bf16[144,2,1024]{2,0,1:T(8,128)(2,1)}), bf16[2304,2,1024]{2,0,1:T(8,128)(2,1)}) %all-gather.5.cloned.1.call-update) | async-done | bytes 9437200 | tf_op jit(solution)/shard_map/all_gather | solution.py:170
  105.8 8.7 %convolution_bitcast_fusion.1 = f32[2304,2,256]{2,0,1:T(8,128)} fusion(bf16[2304,2,1024]{2,0,1:T(8,128)(2,1)} %all-gather.5.cloned.1.call-done, bf16[2,1024,256]{2,1,0:T(8,128)(2,1)} %param.29), kind=kOutput, calls=%fused_computation.26 | convolution fusion | flops 2415919104 | bytes 15204352 | tf_op jit(solution)/shard_map/rjd,jdf->rjf/dot_general | solution.py:127
  114.5 11.7 %convert_bitcast_fusion = bf16[2304,2,1024]{2,0,1:T(8,128)(2,1)} fusion(bf16[2,256,1024]{2,1,0:T(8,128)(2,1)} %param.31, bf16[2304,2,1024]{2,0,1:T(8,128)(2,1)} %all-gather.5.cloned.1.call-done, bf16[2,1024,256]{2,1,0:T(8,128)(2,1)} %param.30, f32[2304,2,256]{2,0,1:T(8,128)} %convolution_bitcast_fusion.1), kind=kOutput, calls=%fused_computation.23 | convolution fusion | flops 4843634688 | bytes 25690112 | tf_op jit(solution)/shard_map/rjf,jfd->rjd/dot_general | solution.py:133
  126.2 36.4 %all-gather.3.cloned.1.call-done = bf16[16384,1,128]{2,0,1:T(8,128)(2,1)} async-done(((bf16[1024,1,128]{2,0,1:T(8,128)(2,1)}), bf16[16384,1,128]{2,0,1:T(8,128)(2,1)}) %all-gather.3.cloned.1.call-update) | async-done | bytes 4194320 | tf_op jit(solution)/shard_map/all_gather | solution.py:115
  162.7 131.4 %while.15 = (s32[]{:T(128)}, f32[1024,1,1]{0,2,1:T(1,128)S(1)}, f32[1024,1,1]{0,2,1:T(1,128)S(1)}, f32[1024,1,1,64]{0,3,2,1:T(8,128)S(1)}, bf16[16,1024,1,128]{3...) while((s32[]{:T(128)}, f32[1024,1,1]{0,2,1:T(1,128)S(1)}, ...), condition=%wide.region_6.7_spmd.clone, body=%wide.region_3.6_spmd.clone.sunk | while | flops 277025792 | bytes 31129728 | solution.py:74
  163.6 2.7 multiply_reduce_fusion.4
  166.4 3.1 fusion.81
  171.7 2.7 multiply_reduce_fusion.4
  174.5 3.2 fusion.81
  180.3 2.7 multiply_reduce_fusion.4
  183.0 3.2 fusion.81
  188.6 2.7 multiply_reduce_fusion.4
  191.3 3.2 fusion.81
  196.9 2.7 multiply_reduce_fusion.4
  199.6 3.2 fusion.81
  205.2 2.7 multiply_reduce_fusion.4
  207.9 3.2 fusion.81
  213.5 2.7 multiply_reduce_fusion.4
  216.2 3.2 fusion.81
  221.8 2.7 multiply_reduce_fusion.4
  224.5 3.2 fusion.81
  230.1 2.7 multiply_reduce_fusion.4
  232.8 3.2 fusion.81
  238.3 2.7 multiply_reduce_fusion.4
  241.1 3.1 fusion.81
  246.4 2.7 multiply_reduce_fusion.4
  249.2 3.1 fusion.81
  254.5 2.7 multiply_reduce_fusion.4
  257.3 3.1 fusion.81
  262.6 2.7 multiply_reduce_fusion.4
  265.4 3.1 fusion.81
  270.7 2.7 multiply_reduce_fusion.4
  273.5 3.1 fusion.81
  278.8 2.7 multiply_reduce_fusion.4
  281.6 3.1 fusion.81
  286.9 2.7 multiply_reduce_fusion.4
  289.7 3.1 fusion.81
  296.4 7.9 %all-to-all-start.1 = ((bf16[16,2,2048]{2,1,0:T(2,128)(2,1)}), bf16[16,2,2048]{2,1,0:T(2,128)(2,1)S(1)}, u32[]{:S(2)}, u32[]{:S(2)}) async-start(bf16[16,2,2048]{2,1,0:T(2,128)(2,1)} %reshape.590), calls=%async_computation.1 | async-start | bytes 262144 | tf_op jit(solution)/shard_map/all_to_all | solution.py:122
  304.7 2.5 copy.149
  307.1 6.0 %all-to-all-done.1 = bf16[16,2,2048]{2,1,0:T(2,128)(2,1)S(1)} async-done(((bf16[16,2,2048]{2,1,0:T(2,128)(2,1)}), bf16[16,2,2048]{2,1,0:T(2,128)(2,1)S(1)}, u32[]{:S(2)}, u32[]{:S(2)}) %all-to-all-start.1) | async-done | bytes 131104 | tf_op jit(solution)/shard_map/all_to_all | solution.py:122
  313.1 4.2 %all-to-all-start.3 = ((bf16[16,9,2,1024]{3,2,1,0:T(2,128)(2,1)}), bf16[16,9,2,1024]{3,2,1,0:T(2,128)(2,1)S(1)}, u32[]{:S(2)}, u32[]{:S(2)}) async-start(bf16[16,9,2,1024]{3,2,1,0:T(2,128)(2,1)} %bitcast.24), calls=%async_computation.4 | async-start | bytes 1179648 | tf_op jit(solution)/shard_map/all_to_all | solution.py:175
  318.8 2.7 fusion.20
  321.5 7.7 %all-to-all-done.3 = bf16[16,9,2,1024]{3,2,1,0:T(2,128)(2,1)S(1)} async-done(((bf16[16,9,2,1024]{3,2,1,0:T(2,128)(2,1)}), bf16[16,9,2,1024]{3,2,1,0:T(2,128)(2,1)S(1)}, u32[]{:S(2)}, u32[]{:S(2)}) %all-to-all-start.3) | async-done | bytes 589856 | tf_op jit(solution)/shard_map/all_to_all | solution.py:175
  330.8 2.4 multiply_reduce_fusion.1
  (201 shorter events, 60.3 us)
Async XLA Ops:
  7.2 28.7 %copy-start = (bf16[1024,1024]{1,0:T(8,128)(2,1)S(1)}, bf16[1024,1024]{1,0:T(8,128)(2,1)}, u32[]{:S(2)}) copy-start(bf16[1024,1024]{1,0:T(8,128)(2,1)} %param.19) | copy-start | bytes 6291460
  7.2 25.5 %copy-start.2 = (bf16[64,1,1024]{2,0,1:T(8,128)(2,1)S(1)}, bf16[64,1,1024]{2,0,1:T(8,128)(2,1)}, u32[]{:S(2)}) copy-start(bf16[64,1,1024]{2,0,1:T(8,128)(2,1)} %param.17) | copy-start | bytes 393220
  7.2 25.7 %copy-start.3 = (f32[1024]{0:T(1024)S(1)}, f32[1024]{0:T(1024)}, u32[]{:S(2)}) copy-start(f32[1024]{0:T(1024)} %param.18) | copy-start | bytes 12292
  7.2 98.6 %all-gather.5.cloned.1.call-start = ((), (), s32[]{:S(2)}) async-start(), calls=%async_computation.6 | async-start | bytes 10027008 | tf_op jit(solution)/shard_map/all_gather | solution.py:170
  32.7 15.4 %copy-start.6 = (f32[64]{0:T(128)S(1)}, f32[64]{0:T(128)}, u32[]{:S(2)}) copy-start(f32[64]{0:T(128)} %param.23) | copy-start | bytes 772
  36.7 39.9 %copy-start.5 = (f32[64]{0:T(128)S(1)}, f32[64]{0:T(128)}, u32[]{:S(2)}) copy-start(f32[64]{0:T(128)} %param.22) | copy-start | bytes 772
  37.7 32.7 %all-to-all-start = ((bf16[64,1,16,192]{3,0,1,2:T(8,128)(2,1)}), bf16[64,1,16,192]{3,0,1,2:T(8,128)(2,1)S(1)}, u32[]{:S(2)}, u32[]{:S(2)}) async-start(bf16[64,1,16,192]{3,0,1,2:T(8,128)(2,1)} %pad_maximum_fusion), calls=%async_computation | async-start | bytes 1048576 | tf_op jit(solution)/shard_map/all_to_all | solution.py:97
  48.1 114.6 %all-gather.3.cloned.1.call-start = ((), (), s32[]{:S(2)}) async-start(), calls=%async_computation.5 | async-start | bytes 4456448 | tf_op jit(solution)/shard_map/all_gather | solution.py:115
  75.1 229.5 %reduce-scatter.2.cloned.1.call-start = ((), (), s32[]{:S(2)}) async-start(), calls=%async_computation.7 | async-start | bytes 10027008 | tf_op jit(solution)/shard_map/reduce_scatter | solution.py:171
  162.7 141.9 %copy-start.4 = (f32[128,2]{0,1:T(2,128)S(1)}, f32[128,2]{0,1:T(2,128)}, u32[]{:S(2)}) copy-start(f32[128,2]{0,1:T(2,128)} %param.28) | copy-start | bytes 3076
  166.4 3.4 %copy-start.1 = (f32[1024,1024]{1,0:T(8,128)S(1)}, f32[1024,1024]{1,0:T(8,128)}, u32[]{:S(2)}) copy-start(f32[1024,1024]{1,0:T(8,128)} %get-tuple-element.163) | copy-start | bytes 12582916 | tf_op jit(solution)/shard_map/while
  174.5 3.9 %copy-start.1 = (f32[1024,1024]{1,0:T(8,128)S(1)}, f32[1024,1024]{1,0:T(8,128)}, u32[]{:S(2)}) copy-start(f32[1024,1024]{1,0:T(8,128)} %get-tuple-element.163) | copy-start | bytes 12582916 | tf_op jit(solution)/shard_map/while
  183.0 3.6 %copy-start.1 = (f32[1024,1024]{1,0:T(8,128)S(1)}, f32[1024,1024]{1,0:T(8,128)}, u32[]{:S(2)}) copy-start(f32[1024,1024]{1,0:T(8,128)} %get-tuple-element.163) | copy-start | bytes 12582916 | tf_op jit(solution)/shard_map/while
  191.3 3.6 %copy-start.1 = (f32[1024,1024]{1,0:T(8,128)S(1)}, f32[1024,1024]{1,0:T(8,128)}, u32[]{:S(2)}) copy-start(f32[1024,1024]{1,0:T(8,128)} %get-tuple-element.163) | copy-start | bytes 12582916 | tf_op jit(solution)/shard_map/while
  199.6 3.6 %copy-start.1 = (f32[1024,1024]{1,0:T(8,128)S(1)}, f32[1024,1024]{1,0:T(8,128)}, u32[]{:S(2)}) copy-start(f32[1024,1024]{1,0:T(8,128)} %get-tuple-element.163) | copy-start | bytes 12582916 | tf_op jit(solution)/shard_map/while
  207.9 3.6 %copy-start.1 = (f32[1024,1024]{1,0:T(8,128)S(1)}, f32[1024,1024]{1,0:T(8,128)}, u32[]{:S(2)}) copy-start(f32[1024,1024]{1,0:T(8,128)} %get-tuple-element.163) | copy-start | bytes 12582916 | tf_op jit(solution)/shard_map/while
  216.2 3.6 %copy-start.1 = (f32[1024,1024]{1,0:T(8,128)S(1)}, f32[1024,1024]{1,0:T(8,128)}, u32[]{:S(2)}) copy-start(f32[1024,1024]{1,0:T(8,128)} %get-tuple-element.163) | copy-start | bytes 12582916 | tf_op jit(solution)/shard_map/while
  224.5 3.6 %copy-start.1 = (f32[1024,1024]{1,0:T(8,128)S(1)}, f32[1024,1024]{1,0:T(8,128)}, u32[]{:S(2)}) copy-start(f32[1024,1024]{1,0:T(8,128)} %get-tuple-element.163) | copy-start | bytes 12582916 | tf_op jit(solution)/shard_map/while
  232.8 3.6 %copy-start.1 = (f32[1024,1024]{1,0:T(8,128)S(1)}, f32[1024,1024]{1,0:T(8,128)}, u32[]{:S(2)}) copy-start(f32[1024,1024]{1,0:T(8,128)} %get-tuple-element.163) | copy-start | bytes 12582916 | tf_op jit(solution)/shard_map/while
  241.0 3.4 %copy-start.1 = (f32[1024,1024]{1,0:T(8,128)S(1)}, f32[1024,1024]{1,0:T(8,128)}, u32[]{:S(2)}) copy-start(f32[1024,1024]{1,0:T(8,128)} %get-tuple-element.163) | copy-start | bytes 12582916 | tf_op jit(solution)/shard_map/while
  249.1 3.4 %copy-start.1 = (f32[1024,1024]{1,0:T(8,128)S(1)}, f32[1024,1024]{1,0:T(8,128)}, u32[]{:S(2)}) copy-start(f32[1024,1024]{1,0:T(8,128)} %get-tuple-element.163) | copy-start | bytes 12582916 | tf_op jit(solution)/shard_map/while
  257.2 3.4 %copy-start.1 = (f32[1024,1024]{1,0:T(8,128)S(1)}, f32[1024,1024]{1,0:T(8,128)}, u32[]{:S(2)}) copy-start(f32[1024,1024]{1,0:T(8,128)} %get-tuple-element.163) | copy-start | bytes 12582916 | tf_op jit(solution)/shard_map/while
  265.4 3.4 %copy-start.1 = (f32[1024,1024]{1,0:T(8,128)S(1)}, f32[1024,1024]{1,0:T(8,128)}, u32[]{:S(2)}) copy-start(f32[1024,1024]{1,0:T(8,128)} %get-tuple-element.163) | copy-start | bytes 12582916 | tf_op jit(solution)/shard_map/while
  273.5 3.4 %copy-start.1 = (f32[1024,1024]{1,0:T(8,128)S(1)}, f32[1024,1024]{1,0:T(8,128)}, u32[]{:S(2)}) copy-start(f32[1024,1024]{1,0:T(8,128)} %get-tuple-element.163) | copy-start | bytes 12582916 | tf_op jit(solution)/shard_map/while
  281.6 3.4 %copy-start.1 = (f32[1024,1024]{1,0:T(8,128)S(1)}, f32[1024,1024]{1,0:T(8,128)}, u32[]{:S(2)}) copy-start(f32[1024,1024]{1,0:T(8,128)} %get-tuple-element.163) | copy-start | bytes 12582916 | tf_op jit(solution)/shard_map/while
  289.7 3.4 %copy-start.1 = (f32[1024,1024]{1,0:T(8,128)S(1)}, f32[1024,1024]{1,0:T(8,128)}, u32[]{:S(2)}) copy-start(f32[1024,1024]{1,0:T(8,128)} %get-tuple-element.163) | copy-start | bytes 12582916 | tf_op jit(solution)/shard_map/while
  296.4 16.8 %all-to-all-start.1 = ((bf16[16,2,2048]{2,1,0:T(2,128)(2,1)}), bf16[16,2,2048]{2,1,0:T(2,128)(2,1)S(1)}, u32[]{:S(2)}, u32[]{:S(2)}) async-start(bf16[16,2,2048]{2,1,0:T(2,128)(2,1)} %reshape.590), calls=%async_computation.1 | async-start | bytes 262144 | tf_op jit(solution)/shard_map/all_to_all | solution.py:122
  313.1 16.1 %all-to-all-start.3 = ((bf16[16,9,2,1024]{3,2,1,0:T(2,128)(2,1)}), bf16[16,9,2,1024]{3,2,1,0:T(2,128)(2,1)S(1)}, u32[]{:S(2)}, u32[]{:S(2)}) async-start(bf16[16,9,2,1024]{3,2,1,0:T(2,128)(2,1)} %bitcast.24), calls=%async_computation.4 | async-start | bytes 1179648 | tf_op jit(solution)/shard_map/all_to_all | solution.py:175
Sparse Core Ops, SparseCore 0:
  32.8 72.8 all-gather.4
  108.2 54.3 all-gather.2
  165.2 69.8 reduce-scatter.1
where the time goes:
time: 341 us; the launch traced here: 340 us
  waiting for transfers between devices  101 us (30%)
  matrix products  85.9 us (25%)
  other arithmetic  61.8 us (18%)
  local copies, waits for them, and re-layouts  35 us (10%)
  starting transfers between devices  22.7 us (7%)
  blocking collectives  18.7 us (5%)
  between operations  14.2 us (4%)
    reduce_sum x16, other arithmetic, step_block(): totals = totals * shrink + jnp.sum(raised, axis=-1)  50 us
    dot_general x16, matrix products, step_block(): jnp.einsum('qshd,ksd->qshk', queries, keys_part, preferred_element_type=j...  43.4 us
    all_gather x1, waiting for transfers between devices, mixer_half(): lax.all_gather(key_pairs, 'ep', axis=0, tiled=True)  36.4 us
    all_gather x1, waiting for transfers between devices, expert_half(): lax.all_gather(incoming, 'tp', axis=0, tiled=True)  28.6 us
    all_to_all x1, waiting for transfers between devices, mixer_half(): lax.all_to_all(packed, 'tp', split_axis=2, concat_axis=0, tiled=True)  22.1 us
    all_to_all x1, blocking collectives, expert_half(): lax.all_to_all(outgoing, 'ep', split_axis=0, concat_axis=0, tiled=True)  18.7 us
    squeeze x16, local copies, waits for them, and re-layouts, attend(): return lax.scan(step_block, fold_state, blocks)[0]  15.6 us
    dot_general x16, matrix products, step_block(): jnp.einsum('qshk,ksd->qshd', raised.astype(jnp.bfloat16), values_part, pr...  14.9 us
  transfers between devices with their start and end apart: 6, of which 5 were waited for; matrix products, arithmetic and copies ran while one was open for 49% of the time, Pallas kernels for 0%

commit v1 on v0

--- a/solution.py
+++ b/solution.py
@@ -167,7 +167,16 @@
     incoming = lax.all_to_all(outgoing, "ep", split_axis=0, concat_axis=0, tiled=True)
     own_rows = ep_count * capacity
     incoming = incoming.reshape(own_rows, local_experts, model_width)
-    hidden_all = joint_hidden(w_gate, w_up, lax.all_gather(incoming, "tp", axis=0, tiled=True))
+    hidden_all = joint_hidden(
+        w_gate,
+        w_up,
+        jnp.concatenate(
+            lax.all_to_all(
+                jnp.stack([incoming for _ in range(lax.axis_size("tp"))], 0), "tp", 0, 0
+            ),
+            0,
+        ),
+    )
     summed = lax.psum_scatter(
         joint_down(hidden_all, w_down).astype(jnp.bfloat16), "tp", scatter_dimension=0, tiled=True
     )

time: 341 us -> 482 us (1.41)
  waiting for transfers between devices: 101 us -> 239 us
  blocking collectives: 18.7 us -> 0 us
  local copies, waits for them, and re-layouts: 35 us -> 47.1 us
  starting transfers between devices: 22.7 us -> 32.6 us
    all_to_all x0 -> x2, waiting for transfers between devices: none -> 208 us  [the longest x1 201 us: expert_half(): lax.all_to_all(jnp.stack([incoming for _ in range(lax.axis_size('tp'))],...]
    all_gather x1, waiting for transfers between devices: 36.4 us -> 0.02 us  [mixer_half(): lax.all_gather(key_pairs, 'ep', axis=0, tiled=True)]
    all_gather x1 -> x0, waiting for transfers between devices: 28.6 us -> none  [expert_half(): lax.all_gather(incoming, 'tp', axis=0, tiled=True)]
    all_to_all x1 -> x0, blocking collectives: 18.7 us -> none  [expert_half(): lax.all_to_all(outgoing, 'ep', split_axis=0, concat_axis=0, tiled=True)]
    all_to_all x0 -> x2, starting transfers between devices: none -> 12.4 us  [the longest x1 7.57 us: expert_half(): lax.all_to_all(outgoing, 'ep', split_axis=0, concat_axis=0, tiled=True)]
    all_to_all x0 -> x1, local copies, waits for them, and re-layouts: none -> 9.14 us  [expert_half(): lax.all_to_all(jnp.stack([incoming for _ in range(lax.axis_size('tp'))],...]
    all_to_all x1, waiting for transfers between devices: 22.1 us -> 17.1 us  [mixer_half(): lax.all_to_all(packed, 'tp', split_axis=2, concat_axis=0, tiled=True)]
    another operation x2 -> x4, local copies, waits for them, and re-layouts: 0.2 us -> 5.2 us  [the longest x2 5 us: expert_half(): jnp.stack([incoming for _ in range(lax.axis_size('tp'))], 0)]
  transfers between devices with their start and end apart: 6 -> 7, of which waited for: 5 -> 5; matrix products, arithmetic and copies ran while one was open for 49% -> 35% of each run, Pallas kernels for 0% -> 0%
where the time goes in v1:
time: 482 us; the launch traced here: 481 us
  waiting for transfers between devices  239 us (50%)
  matrix products  85.4 us (18%)
  other arithmetic  59.9 us (12%)
  local copies, waits for them, and re-layouts  47.1 us (10%)
  starting transfers between devices  32.6 us (7%)
  between operations  16 us (3%)
    all_to_all x1, waiting for transfers between devices, expert_half(): lax.all_to_all(jnp.stack([incoming for _ in range(lax.axis_size('tp'))],...  201 us
    reduce_sum x16, other arithmetic, step_block(): totals = totals * shrink + jnp.sum(raised, axis=-1)  49.7 us
    dot_general x16, matrix products, step_block(): jnp.einsum('qshd,ksd->qshk', queries, keys_part, preferred_element_type=j...  44.1 us
    all_to_all x1, waiting for transfers between devices, mixer_half(): lax.all_to_all(packed, 'tp', split_axis=2, concat_axis=0, tiled=True)  17.1 us
    squeeze x16, local copies, waits for them, and re-layouts, attend(): return lax.scan(step_block, fold_state, blocks)[0]  15.6 us
    dot_general x16, matrix products, step_block(): jnp.einsum('qshk,ksd->qshd', raised.astype(jnp.bfloat16), values_part, pr...  15 us
    dot_general x1, matrix products, joint_down(): jnp.einsum('rjf,jfd->rjd', hidden_all, w_down, preferred_element_type=jnp...  11.6 us
    all_to_all x1, starting transfers between devices, mixer_half(): lax.all_to_all(packed, 'tp', split_axis=2, concat_axis=0, tiled=True)  10.5 us
  transfers between devices with their start and end apart: 7, of which 5 were waited for; matrix products, arithmetic and copies ran while one was open for 35% of the time, Pallas kernels for 0%

profile of v1, /device:TPU:1, one launch (start us, length us, event | category | flops | bytes accessed | tf_op | source)
XLA Modules:
  0.0 480.6 jit_solution(12613687883258034145)
XLA Ops:
  14.7 7.6 %all-to-all-start.2 = ((bf16[16,9,2,1024]{3,2,1,0:T(2,128)(2,1)}), bf16[16,9,2,1024]{3,2,1,0:T(2,128)(2,1)S(1)}, u32[]{:S(2)}, u32[]{:S(2)}) async-start(bf16[16,9,2,1024]{3,2,1,0:T(2,128)(2,1)} %reshape.573), calls=%async_computation.2 | async-start | bytes 1179648 | tf_op jit(solution)/shard_map/all_to_all | solution.py:167
  26.2 7.2 %all-to-all-done.2 = bf16[16,9,2,1024]{3,2,1,0:T(2,128)(2,1)S(1)} async-done(((bf16[16,9,2,1024]{3,2,1,0:T(2,128)(2,1)}), bf16[16,9,2,1024]{3,2,1,0:T(2,128)(2,1)S(1)}, u32[]{:S(2)}, u32[]{:S(2)}) %all-to-all-start.2) | async-done | bytes 589856 | tf_op jit(solution)/shard_map/all_to_all | solution.py:167
  33.4 10.5 %all-to-all-start = ((bf16[64,1,16,192]{3,0,1,2:T(8,128)(2,1)}), bf16[64,1,16,192]{3,0,1,2:T(8,128)(2,1)S(1)}, u32[]{:S(2)}, u32[]{:S(2)}) async-start(bf16[64,1,16,192]{3,0,1,2:T(8,128)(2,1)} %pad_maximum_fusion), calls=%async_computation | async-start | bytes 1048576 | tf_op jit(solution)/shard_map/all_to_all | solution.py:97
  44.0 17.1 %all-to-all-done = bf16[64,1,16,192]{3,0,1,2:T(8,128)(2,1)S(1)} async-done(((bf16[64,1,16,192]{3,0,1,2:T(8,128)(2,1)}), bf16[64,1,16,192]{3,0,1,2:T(8,128)(2,1)S(1)}, u32[]{:S(2)}, u32[]{:S(2)}) %all-to-all-start) | async-done | bytes 393248 | tf_op jit(solution)/shard_map/all_to_all | solution.py:97
  61.1 4.9 %stack.23 = bf16[16,144,2,1024]{3,1,2,0:T(8,128)(2,1)} broadcast(bf16[144,2,1024]{2,0,1:T(8,128)(2,1)S(1)} %copy.151), dimensions={1,2,3} | broadcast | bytes 10027008 | tf_op jit(solution)/shard_map/stack | solution.py:175
  66.0 4.8 %all-to-all-start.3 = ((bf16[16,144,2,1024]{3,1,2,0:T(8,128)(2,1)}), bf16[16,144,2,1024]{3,1,2,0:T(8,128)(2,1)}, u32[]{:S(2)}, u32[]{:S(2)}) async-start(bf16[16,144,2,1024]{3,1,2,0:T(8,128)(2,1)} %stack.23), calls=%async_computation.3 | async-start | bytes 18874368 | tf_op jit(solution)/shard_map/all_to_all | solution.py:174
  74.6 200.8 %all-to-all-done.3 = bf16[16,144,2,1024]{3,1,2,0:T(8,128)(2,1)} async-done(((bf16[16,144,2,1024]{3,1,2,0:T(8,128)(2,1)}), bf16[16,144,2,1024]{3,1,2,0:T(8,128)(2,1)}, u32[]{:S(2)}, u32[]{:S(2)}) %all-to-all-start.3) | async-done | bytes 9437216 | tf_op jit(solution)/shard_map/all_to_all | solution.py:174
  275.3 9.1 %copy.152 = bf16[16,144,2,1024]{3,1,0,2:T(8,128)(2,1)} copy(bf16[16,144,2,1024]{3,1,2,0:T(8,128)(2,1)} %all-to-all-done.3) | data formatting | bytes 18874368 | tf_op jit(solution)/shard_map/all_to_all | solution.py:174
  284.5 8.5 %convolution_bitcast_fusion.1 = f32[2304,2,256]{2,0,1:T(8,128)} fusion(bf16[2304,2,1024]{2,0,1:T(8,128)(2,1)} %bitcast.150, bf16[2,1024,256]{2,1,0:T(8,128)(2,1)S(1)} %copy-done.9), kind=kOutput, calls=%fused_computation.26 | convolution fusion | flops 2415919104 | bytes 15204352 | tf_op jit(solution)/shard_map/rjd,jdf->rjf/dot_general | solution.py:127
  292.9 11.6 %convert_bitcast_fusion = bf16[2304,2,1024]{2,0,1:T(8,128)(2,1)} fusion(bf16[2,256,1024]{2,1,0:T(8,128)(2,1)} %param.31, bf16[2304,2,1024]{2,0,1:T(8,128)(2,1)} %bitcast.151, bf16[2,1024,256]{2,1,0:T(8,128)(2,1)} %param.30, f32[2304,2,256]{2,0,1:T(8,128)} %convolution_bitcast_fusion.1), kind=kOutput, calls=%fused_computation.23 | convolution fusion | flops 4843634688 | bytes 25690112 | tf_op jit(solution)/shard_map/rjf,jfd->rjd/dot_general | solution.py:133
  304.6 131.7 %while.15 = (s32[]{:T(128)}, f32[1024,1,1]{0,2,1:T(1,128)S(1)}, f32[1024,1,1]{0,2,1:T(1,128)S(1)}, f32[1024,1,1,64]{0,3,2,1:T(8,128)S(1)}, bf16[16,1024,1,128]{3...) while((s32[]{:T(128)}, f32[1024,1,1]{0,2,1:T(1,128)S(1)}, ...), condition=%wide.region_6.7_spmd.clone, body=%wide.region_3.6_spmd.clone.sunk | while | flops 277025792 | bytes 31129728 | solution.py:74
  305.6 2.8 multiply_reduce_fusion.4
  308.3 3.1 fusion.81
  313.8 2.8 multiply_reduce_fusion.4
  316.5 3.2 fusion.81
  322.1 2.8 multiply_reduce_fusion.4
  324.9 3.1 fusion.81
  330.4 2.8 multiply_reduce_fusion.4
  333.2 3.2 fusion.81
  338.7 2.8 multiply_reduce_fusion.4
  341.5 3.2 fusion.81
  347.1 2.8 multiply_reduce_fusion.4
  349.8 3.2 fusion.81
  355.4 2.8 multiply_reduce_fusion.4
  358.2 3.2 fusion.81
  363.7 2.8 multiply_reduce_fusion.4
  366.5 3.1 fusion.81
  372.0 2.8 multiply_reduce_fusion.4
  374.8 3.1 fusion.81
  380.2 2.8 multiply_reduce_fusion.4
  382.9 3.1 fusion.81
  388.3 2.8 multiply_reduce_fusion.4
  391.1 3.1 fusion.81
  396.5 2.8 multiply_reduce_fusion.4
  399.2 3.1 fusion.81
  404.6 2.8 multiply_reduce_fusion.4
  407.4 3.1 fusion.81
  412.8 2.8 multiply_reduce_fusion.4
  415.5 3.1 fusion.81
  420.9 2.8 multiply_reduce_fusion.4
  423.7 3.1 fusion.81
  429.1 2.8 multiply_reduce_fusion.4
  431.8 3.1 fusion.81
  438.6 5.6 %all-to-all-start.1 = ((bf16[16,2,2048]{2,1,0:T(2,128)(2,1)}), bf16[16,2,2048]{2,1,0:T(2,128)(2,1)S(1)}, u32[]{:S(2)}, u32[]{:S(2)}) async-start(bf16[16,2,2048]{2,1,0:T(2,128)(2,1)} %reshape.592), calls=%async_computation.1 | async-start | bytes 262144 | tf_op jit(solution)/shard_map/all_to_all | solution.py:122
  447.1 6.0 %all-to-all-done.1 = bf16[16,2,2048]{2,1,0:T(2,128)(2,1)S(1)} async-done(((bf16[16,2,2048]{2,1,0:T(2,128)(2,1)}), bf16[16,2,2048]{2,1,0:T(2,128)(2,1)S(1)}, u32[]{:S(2)}, u32[]{:S(2)}) %all-to-all-start.1) | async-done | bytes 131104 | tf_op jit(solution)/shard_map/all_to_all | solution.py:122
  453.0 3.8 all-to-all-start.4
  458.4 2.9 fusion.20
  461.2 7.9 %all-to-all-done.4 = bf16[16,9,2,1024]{3,2,1,0:T(2,128)(2,1)S(1)} async-done(((bf16[16,9,2,1024]{3,2,1,0:T(2,128)(2,1)}), bf16[16,9,2,1024]{3,2,1,0:T(2,128)(2,1)S(1)}, u32[]{:S(2)}, u32[]{:S(2)}) %all-to-all-start.4) | async-done | bytes 589856 | tf_op jit(solution)/shard_map/all_to_all | solution.py:184
  (209 shorter events, 62.0 us)
Async XLA Ops:
  8.0 16.3 %copy-start = (bf16[1024,1024]{1,0:T(8,128)(2,1)S(1)}, bf16[1024,1024]{1,0:T(8,128)(2,1)}, u32[]{:S(2)}) copy-start(bf16[1024,1024]{1,0:T(8,128)(2,1)} %param.19) | copy-start | bytes 6291460
  8.0 14.2 %copy-start.3 = (bf16[64,1,1024]{2,0,1:T(8,128)(2,1)S(1)}, bf16[64,1,1024]{2,0,1:T(8,128)(2,1)}, u32[]{:S(2)}) copy-start(bf16[64,1,1024]{2,0,1:T(8,128)(2,1)} %param.17) | copy-start | bytes 393220
  8.0 14.4 %copy-start.5 = (f32[1024]{0:T(1024)S(1)}, f32[1024]{0:T(1024)}, u32[]{:S(2)}) copy-start(f32[1024]{0:T(1024)} %param.18) | copy-start | bytes 12292
  8.0 14.4 %copy-start.4 = (bf16[1024,256]{1,0:T(8,128)(2,1)S(1)}, bf16[1024,256]{1,0:T(8,128)(2,1)}, u32[]{:S(2)}) copy-start(bf16[1024,256]{1,0:T(8,128)(2,1)} %param.20) | copy-start | bytes 1572868
  14.7 18.7 %all-to-all-start.2 = ((bf16[16,9,2,1024]{3,2,1,0:T(2,128)(2,1)}), bf16[16,9,2,1024]{3,2,1,0:T(2,128)(2,1)S(1)}, u32[]{:S(2)}, u32[]{:S(2)}) async-start(bf16[16,9,2,1024]{3,2,1,0:T(2,128)(2,1)} %reshape.573), calls=%async_computation.2 | async-start | bytes 1179648 | tf_op jit(solution)/shard_map/all_to_all | solution.py:167
  33.4 27.7 %all-to-all-start = ((bf16[64,1,16,192]{3,0,1,2:T(8,128)(2,1)}), bf16[64,1,16,192]{3,0,1,2:T(8,128)(2,1)S(1)}, u32[]{:S(2)}, u32[]{:S(2)}) async-start(bf16[64,1,16,192]{3,0,1,2:T(8,128)(2,1)} %pad_maximum_fusion), calls=%async_computation | async-start | bytes 1048576 | tf_op jit(solution)/shard_map/all_to_all | solution.py:97
  66.0 4.9 %copy-start.8 = (f32[64]{0:T(128)S(1)}, f32[64]{0:T(128)}, u32[]{:S(2)}) copy-start(f32[64]{0:T(128)} %param.23) | copy-start | bytes 772
  66.0 209.4 %all-to-all-start.3 = ((bf16[16,144,2,1024]{3,1,2,0:T(8,128)(2,1)}), bf16[16,144,2,1024]{3,1,2,0:T(8,128)(2,1)}, u32[]{:S(2)}, u32[]{:S(2)}) async-start(bf16[16,144,2,1024]{3,1,2,0:T(8,128)(2,1)} %stack.23), calls=%async_computation.3 | async-start | bytes 18874368 | tf_op jit(solution)/shard_map/all_to_all | solution.py:174
  70.8 3.1 copy-start.7
  70.8 233.7 %all-gather.2.cloned.1.call-start = ((), (), s32[]{:S(2)}) async-start(), calls=%async_computation.6 | async-start | bytes 4456448 | tf_op jit(solution)/shard_map/all_gather | solution.py:115
  73.4 371.1 %reduce-scatter.2.cloned.1.call-start = ((), (), s32[]{:S(2)}) async-start(), calls=%async_computation.7 | async-start | bytes 10027008 | tf_op jit(solution)/shard_map/reduce_scatter | solution.py:180
  74.6 209.9 %copy-start.9 = (bf16[2,1024,256]{2,1,0:T(8,128)(2,1)S(1)}, bf16[2,1024,256]{2,1,0:T(8,128)(2,1)}, u32[]{:S(2)}) copy-start(bf16[2,1024,256]{2,1,0:T(8,128)(2,1)} %param.29) | copy-start | bytes 3145732
  304.6 139.9 %copy-start.6 = (f32[128,2]{0,1:T(2,128)S(1)}, f32[128,2]{0,1:T(2,128)}, u32[]{:S(2)}) copy-start(f32[128,2]{0,1:T(2,128)} %param.28) | copy-start | bytes 3076
  308.3 3.5 copy-start.2
  316.5 3.6 copy-start.2
  324.9 3.6 copy-start.2
  333.2 3.6 copy-start.2
  341.5 3.6 copy-start.2
  349.8 3.6 copy-start.2
  358.2 3.6 copy-start.2
  366.5 3.6 copy-start.2
  374.8 3.4 copy-start.2
  382.9 3.4 copy-start.2
  391.1 3.4 copy-start.2
  399.2 3.4 copy-start.2
  407.4 3.4 copy-start.2
  415.5 3.4 copy-start.2
  423.7 3.4 copy-start.2
  431.8 3.4 copy-start.2
  438.6 14.5 %all-to-all-start.1 = ((bf16[16,2,2048]{2,1,0:T(2,128)(2,1)}), bf16[16,2,2048]{2,1,0:T(2,128)(2,1)S(1)}, u32[]{:S(2)}, u32[]{:S(2)}) async-start(bf16[16,2,2048]{2,1,0:T(2,128)(2,1)} %reshape.592), calls=%async_computation.1 | async-start | bytes 262144 | tf_op jit(solution)/shard_map/all_to_all | solution.py:122
  453.0 16.1 %all-to-all-start.4 = ((bf16[16,9,2,1024]{3,2,1,0:T(2,128)(2,1)}), bf16[16,9,2,1024]{3,2,1,0:T(2,128)(2,1)S(1)}, u32[]{:S(2)}, u32[]{:S(2)}) async-start(bf16[16,9,2,1024]{3,2,1,0:T(2,128)(2,1)} %bitcast.25), calls=%async_computation.5 | async-start | bytes 1179648 | tf_op jit(solution)/shard_map/all_to_all | solution.py:184
  458.3 14.8 %copy-start.1 = (bf16[1024,1024]{1,0:T(8,128)(2,1)S(1)}, bf16[1024,1024]{1,0:T(8,128)(2,1)}, u32[]{:S(2)}) copy-start(bf16[1024,1024]{1,0:T(8,128)(2,1)} %param.19) | copy-start | bytes 6291460
Sparse Core Ops, SparseCore 0:
  74.6 52.0 all-gather.1
Sparse Core Ops, SparseCore 1:
  304.6 65.5 reduce-scatter.1
